TPU v7x, 32 devices: a whole 2x2x4 slice. The times are simulated.
32 devices in a mesh: sp: 8 (over z, x), tp: 4 (over y, core).
Axes of the slice: x: 2, y: 2, z: 4, core: 2. Of those that a mesh axis runs over, the one named last changes fastest.
Arguments:
- cotangent: bfloat16 [1024, 2048], P('sp'), may hold values from -6 to 6
- stream: bfloat16 [1024, 2048], P('sp'), may hold values from -6 to 6
- routes: int32 [1024, 2], P('sp'), may hold values from 0 to 3, all different within a row; in each aligned block of 128 rows (0 to 127, 128 to 255, ...) at most 96 rows name the same one
- route_weights: float32 [1024, 2], P('sp'), may hold values from 0.25 to 1
- gate_weight: bfloat16 [8, 2048, 2048], P('sp', None, 'tp'), may hold values from -0.125 to 0.125
- up_weight: bfloat16 [8, 2048, 2048], P('sp', None, 'tp'), may hold values from -0.125 to 0.125
- down_weight: bfloat16 [8, 2048, 2048], P('sp', 'tp'), may hold values from -0.09375 to 0.09375
- outer_gate: bfloat16 [1024, 1024], P('sp', 'tp'), may hold values from -6 to 6
- inner_gate: bfloat16 [1024, 1024], P('sp', 'tp'), may hold values from -6 to 6
- conv_input: bfloat16 [1024, 1024], P('sp', 'tp'), may hold values from -6 to 6
- conv_taps: bfloat16 [3, 1024], P(None, 'tp'), may hold values from -1 to 1
- out_weight: bfloat16 [2048, 1024], P(None, 'tp'), may hold values from -0.1875 to 0.1875
Outputs:
- gate_grad: bfloat16 [8, 2048, 2048], P('sp', None, 'tp')
- up_grad: bfloat16 [8, 2048, 2048], P('sp', None, 'tp')
- down_grad: bfloat16 [8, 2048, 2048], P('sp', 'tp')
- out_grad: float32 [2048, 1024], P('sp', 'tp')
- outer_grad: bfloat16 [1024, 1024], P('sp', 'tp')
- inner_grad: bfloat16 [1024, 1024], P('sp', 'tp')
- input_grad: bfloat16 [1024, 1024], P('sp', 'tp')
Inputs may be any that keep to these rules, and one draw needn't show every extreme that they name: `routes`: each token names two different experts. Among the 128 tokens of one index of sp no expert is named by more than 96 tokens, a bound that some block of them reaches in every draw.
All inputs are finite; a program needn't handle non-finite values.
Results may differ from a plain program's by a relative error of at most 0.02.
Values may be sent and summed in bfloat16 or wider, within the bound.
A program may use at most 64 MiB of HBM per device.

v0:
```python
import jax
import jax.numpy as jnp
from jax import lax
from jax.sharding import PartitionSpec as P


def from_behind(block, axis, distance):
    devices = range(lax.axis_size(axis))
    route = [(i - distance, i) for i in devices if i - distance in devices]
    return lax.ppermute(block, axis, route)


def per_device(
    cotangent,
    stream,
    routes,
    route_weights,
    gate_weight,
    up_weight,
    down_weight,
    outer_gate,
    inner_gate,
    conv_input,
    conv_taps,
    out_weight,
):
    groups = lax.axis_size("sp")
    tp_count = lax.axis_size("tp")
    experts = groups // 2
    tok_rows = stream.shape[0]
    model_width = stream.shape[1]
    capacity = 3 * tok_rows // experts
    slot_total = experts * capacity
    contract_first = (((0,), (0,)), ((), ()))
    contract_last = (((1,), (1,)), ((), ()))
    flat_routes = routes.reshape(-1)
    choose = (flat_routes[:, None] == jnp.arange(experts, dtype=jnp.int32)[None, :]).astype(
        jnp.int32
    )
    before = jnp.cumsum(choose, axis=0) - choose
    slot_place = flat_routes * capacity + jnp.sum(before * choose, axis=1)
    slot_table = (jnp.arange(slot_total, dtype=jnp.int32)[:, None] == slot_place[None, :]).astype(
        jnp.float32
    )
    select = jnp.sum(slot_table.reshape(slot_total, tok_rows, 2), axis=2).astype(jnp.bfloat16)
    slot_weight = jnp.sum(slot_table * route_weights.reshape(-1)[None, :], axis=1)
    block_width = model_width // tp_count
    offset = lax.axis_index("tp") * block_width
    rows_part = lax.dynamic_slice_in_dim(stream, offset, block_width, 1)
    cot_part = lax.dynamic_slice_in_dim(cotangent, offset, block_width, 1)
    sent_rows = jnp.dot(select, rows_part, preferred_element_type=jnp.float32).astype(jnp.bfloat16)
    sent_cot = (
        jnp.dot(select, cot_part, preferred_element_type=jnp.float32) * slot_weight[:, None]
    ).astype(jnp.bfloat16)
    sent_rows = jnp.repeat(sent_rows.reshape(experts, capacity, -1), 2, axis=0)
    sent_cot = jnp.repeat(sent_cot.reshape(experts, capacity, -1), 2, axis=0)
    recv_rows, recv_cot = (
        lax.all_to_all(sent_rows, "sp", split_axis=0, concat_axis=0, tiled=True),
        lax.all_to_all(sent_cot, "sp", split_axis=0, concat_axis=0, tiled=True),
    )
    recv_rows, recv_cot = (
        lax.all_gather(recv_rows, "tp", axis=2, tiled=True),
        lax.all_gather(recv_cot, "tp", axis=2, tiled=True),
    )
    slots = groups * capacity
    routed_rows = recv_rows.reshape(slots, model_width)
    routed_cot = recv_cot.reshape(slots, model_width)
    gate_local = gate_weight[0]
    up_local = up_weight[0]
    down_local = down_weight[0]
    gate_pre = jnp.dot(routed_rows, gate_local, preferred_element_type=jnp.float32)
    up_pre = jnp.dot(routed_rows, up_local, preferred_element_type=jnp.float32)
    hidden_grad = lax.dot_general(
        routed_cot, down_local, contract_last, preferred_element_type=jnp.float32
    )
    sigma = jax.nn.sigmoid(gate_pre)
    silu_gate = gate_pre * sigma
    hidden = (silu_gate * up_pre).astype(jnp.bfloat16)
    up_delta = (hidden_grad * silu_gate).astype(jnp.bfloat16)
    gate_delta = (hidden_grad * up_pre * sigma * (1.0 + gate_pre * (1.0 - sigma))).astype(
        jnp.bfloat16
    )
    gate_grad = lax.dot_general(
        routed_rows, gate_delta, contract_first, preferred_element_type=jnp.float32
    ).astype(jnp.bfloat16)[None]
    up_grad = lax.dot_general(
        routed_rows, up_delta, contract_first, preferred_element_type=jnp.float32
    ).astype(jnp.bfloat16)[None]
    down_grad = lax.dot_general(
        hidden, routed_cot, contract_first, preferred_element_type=jnp.float32
    ).astype(jnp.bfloat16)[None]
    row_partial = lax.dot_general(
        gate_delta, gate_local, contract_last, preferred_element_type=jnp.float32
    )
    row_partial = row_partial + lax.dot_general(
        up_delta, up_local, contract_last, preferred_element_type=jnp.float32
    )
    half_sums = lax.psum_scatter(
        row_partial.astype(jnp.bfloat16), "tp", scatter_dimension=1, tiled=True
    ).astype(jnp.float32)
    block_width = half_sums.shape[1]
    half_grad = half_sums.reshape(groups, capacity, block_width).astype(jnp.bfloat16)
    returned = lax.all_to_all(half_grad, "sp", split_axis=0, concat_axis=0, tiled=True)
    returned = returned.reshape(experts, 2, capacity, block_width)
    select_three = select.reshape(experts, capacity, tok_rows)
    moe_part = jnp.einsum(
        "ecr,emcd->rd", select_three, returned, preferred_element_type=jnp.float32
    ).astype(jnp.bfloat16)
    moe_grad = lax.all_gather(moe_part, "tp", axis=1, tiled=True)
    stream_grad = (cotangent.astype(jnp.float32) + moe_grad.astype(jnp.float32)).astype(
        jnp.bfloat16
    )
    taps = conv_taps.astype(jnp.float32)
    outer_f = outer_gate.astype(jnp.float32)
    inner_f = inner_gate.astype(jnp.float32)
    input_f = conv_input.astype(jnp.float32)
    mixed = inner_f * input_f
    earlier = from_behind(mixed[-2:], "sp", 1)
    padded = jnp.concatenate([earlier, mixed], axis=0)
    conv_sum = taps[0] * padded[:-2] + taps[1] * padded[1:-1] + taps[2] * padded[2:]
    conv_out = (outer_f * conv_sum).astype(jnp.bfloat16)
    out_grad = lax.psum_scatter(
        lax.dot_general(
            stream_grad, conv_out, contract_first, preferred_element_type=jnp.float32
        ).astype(jnp.bfloat16),
        "sp",
        scatter_dimension=0,
        tiled=True,
    ).astype(jnp.float32)
    conv_grad = jnp.dot(stream_grad, out_weight, preferred_element_type=jnp.float32)
    outer_grad = (conv_grad * conv_sum).astype(jnp.bfloat16)
    scaled = conv_grad * outer_f
    later = from_behind(scaled[:2], "sp", -1)
    extended = jnp.concatenate([scaled, later], axis=0)
    mixed_grad = taps[2] * extended[:-2] + taps[1] * extended[1:-1] + taps[0] * extended[2:]
    inner_grad = (mixed_grad * input_f).astype(jnp.bfloat16)
    input_grad = (mixed_grad * inner_f).astype(jnp.bfloat16)
    return (gate_grad, up_grad, down_grad, out_grad, outer_grad, inner_grad, input_grad)


def solution(mesh):
    placed = (
        P("sp", None),
        P("sp", None),
        P("sp", None),
        P("sp", None),
        P("sp", None, "tp"),
        P("sp", None, "tp"),
        P("sp", "tp", None),
        P("sp", "tp"),
        P("sp", "tp"),
        P("sp", "tp"),
        P(None, "tp"),
        P(None, "tp"),
    )
    return jax.shard_map(
        per_device,
        mesh=mesh,
        in_specs=placed,
        out_specs=(
            P("sp", None, "tp"),
            P("sp", None, "tp"),
            P("sp", "tp", None),
            P("sp", "tp"),
            P("sp", "tp"),
            P("sp", "tp"),
            P("sp", "tp"),
        ),
        check_vma=False,
    )
```

profile of v0, /device:TPU:0, one launch (start us, length us, event | category | flops | bytes accessed | tf_op | source)
XLA Modules:
  0.0 253.2 jit_solution(881290032400397519)
XLA Ops:
  7.2 0.9 copy.37
  8.5 1.2 reduce-window.6
  10.3 0.7 multiply_add_fusion.1
  11.1 1.2 convolution_convert_fusion.4
  12.4 27.3 %all_to_all.15 = bf16[8,96,512]{2,1,0:T(8,128)(2,1)} all-to-all(bf16[8,96,512]{2,1,0:T(8,128)(2,1)S(1)} %bitcast.73), channel_id=1, replica_groups=mesh['sp'=8,'tp'=4] {'sp'}, dimensions={0} | all-to-all | bytes 1572864 | tf_op jit(solution)/shard_map/all_to_all | solution.py:58
  40.2 0.3 fusion.13
  40.6 23.3 %all_to_all.16 = bf16[8,96,512]{2,1,0:T(8,128)(2,1)} all-to-all(bf16[8,96,512]{2,1,0:T(8,128)(2,1)S(1)} %bitcast.74), channel_id=1, replica_groups=mesh['sp'=8,'tp'=4] {'sp'}, dimensions={0} | all-to-all | bytes 1572864 | tf_op jit(solution)/shard_map/all_to_all | solution.py:59
  63.9 3.5 %all-gather.3.cloned.1.call-done = bf16[8,96,2048]{2,1,0:T(8,128)(2,1)} async-done(((bf16[8,96,512]{2,1,0:T(8,128)(2,1)}), bf16[8,96,2048]{2,1,0:T(8,128)(2,1)}) %all-gather.3.cloned.1.call-update) | async-done | bytes 3145744 | tf_op jit(solution)/shard_map/all_gather | solution.py:62
  67.4 5.0 %fusion.5 = f32[768,512]{1,0:T(8,128)} fusion(bf16[768,2048]{1,0:T(8,128)(2,1)} %bitcast.86, bf16[1,2048,512]{2,1,0:T(8,128)(2,1)S(1)} %copy-done), kind=kOutput, calls=%fused_computation.10 | convolution fusion | flops 1610612736 | bytes 6815744 | tf_op jit(solution)/shard_map/dot_general | solution.py:71
  72.4 2.9 %fusion.8 = f32[768,512]{1,0:T(8,128)} fusion(bf16[768,2048]{1,0:T(8,128)(2,1)S(1)} %bitcast.88, bf16[1,2048,512]{2,1,0:T(8,128)(2,1)S(1)} %copy-done.2), kind=kOutput, calls=%fused_computation.13 | convolution fusion | flops 1610612736 | bytes 6815744 | tf_op jit(solution)/shard_map/dot_general | solution.py:72
  75.3 22.2 %all-gather.5.cloned.1.call-done = bf16[8,96,2048]{2,1,0:T(8,128)(2,1)} async-done(((bf16[8,96,512]{2,1,0:T(8,128)(2,1)}), bf16[8,96,2048]{2,1,0:T(8,128)(2,1)}) %all-gather.5.cloned.1.call-update) | async-done | bytes 3145744 | tf_op jit(solution)/shard_map/all_gather | solution.py:63
  97.5 5.7 %multiply_convert_fusion.1 = (bf16[768,512]{1,0:T(8,128)(2,1)S(1)}, bf16[768,512]{1,0:T(8,128)(2,1)S(1)}) fusion(f32[768,512]{1,0:T(8,128)} %fusion.5, f32[768,512]{1,0:T(8,128)} %fusion.8, bf16[768,2048]{1,0:T(8,128)(2,1)} %bitcast.90, bf16[1,512,2048]{2,1,0:T(8,128)(2,1)} %param.18), kind=kOutput, calls=%fused_computation.19 | convolution fusion | flops 1615724544 | bytes 9961472 | tf_op jit(solution)/shard_map/dot_general | solution.py:73
  103.3 1.8 fusion.3
  105.1 0.3 copy-done.3
  105.4 3.5 %add_convert_fusion = bf16[768,2048]{1,0:T(8,128)(2,1)} fusion(f32[768,2048]{1,0:T(8,128)S(1)} %fusion.3, bf16[768,512]{1,0:T(8,128)(2,1)S(1)} %get-tuple-element.11, bf16[1,2048,512]{2,1,0:T(8,128)(2,1)S(1)} %copy-done.3), kind=kOutput, calls=%fused_computation | convolution fusion | flops 1613758464 | bytes 12320768 | tf_op jit(solution)/shard_map/dot_general | solution.py:95
  109.0 37.9 %reduce-scatter.3.cloned.1.call-done = bf16[768,512]{1,0:T(8,128)(2,1)} async-done(((bf16[768,2048]{1,0:T(8,128)(2,1)}), bf16[768,512]{1,0:T(8,128)(2,1)}) %reduce-scatter.3.cloned.1.call-update) | async-done | bytes 786448 | tf_op jit(solution)/shard_map/reduce_scatter | solution.py:98
  146.8 5.5 %all-to-all-start.2 = ((bf16[8,96,512]{2,1,0:T(8,128)(2,1)}), bf16[8,96,512]{2,1,0:T(8,128)(2,1)S(1)}, u32[]{:S(2)}, u32[]{:S(2)}) async-start(bf16[8,96,512]{2,1,0:T(8,128)(2,1)} %bitcast.78), calls=%async_computation.3 | async-start | bytes 1572864 | tf_op jit(solution)/shard_map/all_to_all | solution.py:103
  152.4 0.9 convert_multiply_fusion.1
  153.3 3.9 %collective-permute-start = (f32[2,256]{1,0:T(2,128)S(1)}, f32[2,256]{1,0:T(2,128)S(1)}, u32[]{:S(2)}, u32[]{:S(2)}) collective-permute-start(f32[2,256]{1,0:T(2,128)S(1)} %slice.49), channel_id=1, source_target_pairs={{0,4},{4,8},{8,12},{12,16},{16,20},{20,24},{24,28},{1,5},{5,9},{9,... | collective-permute-start | bytes 6152 | tf_op jit(solution)/shard_map/ppermute | solution.py:10
  157.2 15.2 %all-to-all-done.2 = bf16[8,96,512]{2,1,0:T(8,128)(2,1)S(1)} async-done(((bf16[8,96,512]{2,1,0:T(8,128)(2,1)}), bf16[8,96,512]{2,1,0:T(8,128)(2,1)S(1)}, u32[]{:S(2)}, u32[]{:S(2)}) %all-to-all-start.2) | async-done | bytes 786464 | tf_op jit(solution)/shard_map/all_to_all | solution.py:103
  172.8 6.7 %all_gather.11 = bf16[128,2048]{1,0:T(8,128)(2,1)S(1)} all-gather(bf16[128,512]{1,0:T(8,128)(2,1)S(1)} %fusion.14), channel_id=1, replica_groups=mesh['sp'=8,'tp'=4] {'tp'}, dimensions={1}, use_global_device_ids=true | all-gather | bytes 655360 | tf_op jit(solution)/shard_map/all_gather | solution.py:109
  179.5 1.0 multiply_convert_fusion.4
  180.5 1.5 convolution_convert_fusion.3
  182.1 5.2 %fusion = bf16[1,2048,512]{2,1,0:T(8,128)(2,1)} fusion(bf16[768,2048]{1,0:T(8,128)(2,1)} %bitcast.87, bf16[768,512]{1,0:T(8,128)(2,1)S(1)} %copy-done.8), kind=kOutput, calls=%fused_computation.4 | convolution fusion | flops 1611661312 | bytes 6029312 | tf_op jit(solution)/shard_map/dot_general | solution.py:83
  187.3 3.3 %fusion.2 = bf16[1,512,2048]{2,1,0:T(8,128)(2,1)} fusion(bf16[768,2048]{1,0:T(8,128)(2,1)S(1)} %bitcast.91, f32[768,512]{1,0:T(8,128)S(1)} %copy-done.21, f32[768,512]{1,0:T(8,128)S(1)} %copy-done.20), kind=kOutput, calls=%fused_computation.6 | convolution fusion | flops 1614020608 | bytes 8388608 | tf_op jit(solution)/shard_map/dot_general | solution.py:89
  190.6 1.4 collective-permute-start.1
  192.1 3.2 %fusion.1 = bf16[1,2048,512]{2,1,0:T(8,128)(2,1)} fusion(bf16[768,2048]{1,0:T(8,128)(2,1)S(1)} %bitcast.89, bf16[768,512]{1,0:T(8,128)(2,1)S(1)} %copy-done.6), kind=kOutput, calls=%fused_computation.5 | convolution fusion | flops 1611661312 | bytes 6029312 | tf_op jit(solution)/shard_map/dot_general | solution.py:86
  195.3 1.0 collective-permute-done.1
  196.2 0.7 fusion.26
  196.9 0.6 fusion.27
  197.6 47.4 %reduce-scatter.5.cloned.1.call-done = bf16[256,256]{1,0:T(8,128)(2,1)} async-done(((bf16[2048,256]{1,0:T(8,128)(2,1)}), bf16[256,256]{1,0:T(8,128)(2,1)}) %reduce-scatter.5.cloned.1.call-update) | async-done | bytes 131088 | tf_op jit(solution)/shard_map/reduce_scatter | solution.py:122
  245.0 1.6 convert_element_type.125
  (76 shorter events, 2.2 us)
Async XLA Ops:
  7.2 60.3 %copy-start = (bf16[1,2048,512]{2,1,0:T(8,128)(2,1)S(1)}, bf16[1,2048,512]{2,1,0:T(8,128)(2,1)}, u32[]{:S(2)}) copy-start(bf16[1,2048,512]{2,1,0:T(8,128)(2,1)} %param.16) | copy-start | bytes 6291460
  7.2 60.3 %all-gather.3.cloned.1.call-start = ((), (), s32[]{:S(2)}) async-start(), calls=%async_computation.5 | async-start | bytes 3932160 | tf_op jit(solution)/shard_map/all_gather | solution.py:62
  11.1 28.7 %copy-start.16 = (f32[128,2]{0,1:T(2,128)S(1)}, f32[128,2]{0,1:T(2,128)}, u32[]{:S(2)}) copy-start(f32[128,2]{0,1:T(2,128)} %param.15) | copy-start | bytes 3076
  11.1 29.1 %copy-start.1 = (bf16[128,2048]{1,0:T(8,128)(2,1)S(1)}, bf16[128,2048]{1,0:T(8,128)(2,1)}, u32[]{:S(2)}) copy-start(bf16[128,2048]{1,0:T(8,128)(2,1)} %param.12) | copy-start | bytes 1572868
  39.7 57.8 %all-gather.5.cloned.1.call-start = ((), (), s32[]{:S(2)}) async-start(), calls=%async_computation.6 | async-start | bytes 3932160 | tf_op jit(solution)/shard_map/all_gather | solution.py:63
  63.9 83.0 %reduce-scatter.3.cloned.1.call-start = ((), (), s32[]{:S(2)}) async-start(), calls=%async_computation.7 | async-start | bytes 3932160 | tf_op jit(solution)/shard_map/reduce_scatter | solution.py:98
  67.4 5.0 %copy-start.2 = (bf16[1,2048,512]{2,1,0:T(8,128)(2,1)S(1)}, bf16[1,2048,512]{2,1,0:T(8,128)(2,1)}, u32[]{:S(2)}) copy-start(bf16[1,2048,512]{2,1,0:T(8,128)(2,1)} %param.17) | copy-start | bytes 6291460
  67.4 5.0 %copy-start.17 = (bf16[8,96,2048]{2,1,0:T(8,128)(2,1)S(1)}, bf16[8,96,2048]{2,1,0:T(8,128)(2,1)}, u32[]{:S(2)}) copy-start(bf16[8,96,2048]{2,1,0:T(8,128)(2,1)} %all-gather.3.cloned.1.call-done) | copy-start | bytes 9437188
  103.2 1.9 copy-start.7
  103.2 1.9 copy-start.5
  103.3 2.2 copy-start.3
  108.9 48.3 %copy-start.15 = (bf16[3,256]{1,0:T(4,128)(2,1)S(1)}, bf16[3,256]{1,0:T(4,128)(2,1)}, u32[]{:S(2)}) copy-start(bf16[3,256]{1,0:T(4,128)(2,1)} %param.22) | copy-start | bytes 4612
  146.8 25.6 %all-to-all-start.2 = ((bf16[8,96,512]{2,1,0:T(8,128)(2,1)}), bf16[8,96,512]{2,1,0:T(8,128)(2,1)S(1)}, u32[]{:S(2)}, u32[]{:S(2)}) async-start(bf16[8,96,512]{2,1,0:T(8,128)(2,1)} %bitcast.78), calls=%async_computation.3 | async-start | bytes 1572864 | tf_op jit(solution)/shard_map/all_to_all | solution.py:103
  152.4 92.7 %reduce-scatter.5.cloned.1.call-start = ((), (), s32[]{:S(2)}) async-start(), calls=%async_computation.8 | async-start | bytes 1179648 | tf_op jit(solution)/shard_map/reduce_scatter | solution.py:122
  153.3 3.9 %copy-start.10 = (f32[128,256]{1,0:T(8,128)}, f32[128,256]{1,0:T(8,128)S(1)}, u32[]{:S(2)}) copy-start(f32[128,256]{1,0:T(8,128)S(1)} %convert_multiply_fusion.1) | copy-start | bytes 393220
  153.3 26.2 %collective-permute-start = (f32[2,256]{1,0:T(2,128)S(1)}, f32[2,256]{1,0:T(2,128)S(1)}, u32[]{:S(2)}, u32[]{:S(2)}) collective-permute-start(f32[2,256]{1,0:T(2,128)S(1)} %slice.49), channel_id=1, source_target_pairs={{0,4},{4,8},{8,12},{12,16},{16,20},{20,24},{24,28},{1,5},{5,9},{9,... | collective-permute-start | bytes 6152 | tf_op jit(solution)/shard_map/ppermute | solution.py:10
  172.4 7.1 %copy-start.4 = (bf16[2048,256]{1,0:T(8,128)(2,1)S(1)}, bf16[2048,256]{1,0:T(8,128)(2,1)}, u32[]{:S(2)}) copy-start(bf16[2048,256]{1,0:T(8,128)(2,1)} %param.23) | copy-start | bytes 3145732
  172.4 7.1 %copy-start.11 = (f32[128,256]{1,0:T(8,128)S(1)}, f32[128,256]{1,0:T(8,128)}, u32[]{:S(2)}) copy-start(f32[128,256]{1,0:T(8,128)} %copy-done.10) | copy-start | bytes 393220
  172.4 7.1 %copy-start.12 = (bf16[128,256]{1,0:T(8,128)(2,1)S(1)}, bf16[128,256]{1,0:T(8,128)(2,1)}, u32[]{:S(2)}) copy-start(bf16[128,256]{1,0:T(8,128)(2,1)} %param.19) | copy-start | bytes 196612
  180.5 1.5 copy-start.8
  182.0 5.2 %copy-start.19 = (bf16[8,96,2048]{2,1,0:T(8,128)(2,1)S(1)}, bf16[8,96,2048]{2,1,0:T(8,128)(2,1)}, u32[]{:S(2)}) copy-start(bf16[8,96,2048]{2,1,0:T(8,128)(2,1)} %all-gather.5.cloned.1.call-done) | copy-start | bytes 9437188
  182.0 5.2 %copy-start.20 = (f32[768,512]{1,0:T(8,128)S(1)}, f32[768,512]{1,0:T(8,128)}, u32[]{:S(2)}) copy-start(f32[768,512]{1,0:T(8,128)} %fusion.5) | copy-start | bytes 4718596
  182.1 5.2 %copy-start.21 = (f32[768,512]{1,0:T(8,128)S(1)}, f32[768,512]{1,0:T(8,128)}, u32[]{:S(2)}) copy-start(f32[768,512]{1,0:T(8,128)} %fusion.8) | copy-start | bytes 4718596
  187.3 3.3 %copy-start.9 = (f32[128,256]{1,0:T(8,128)S(1)}, f32[128,256]{1,0:T(8,128)}, u32[]{:S(2)}) copy-start(f32[128,256]{1,0:T(8,128)} %get-tuple-element.13) | copy-start | bytes 393220
  187.3 4.8 %copy-start.6 = (bf16[768,512]{1,0:T(8,128)(2,1)S(1)}, bf16[768,512]{1,0:T(8,128)(2,1)}, u32[]{:S(2)}) copy-start(bf16[768,512]{1,0:T(8,128)(2,1)} %copy-done.5) | copy-start | bytes 2359300
  187.3 4.8 %copy-start.18 = (bf16[8,96,2048]{2,1,0:T(8,128)(2,1)S(1)}, bf16[8,96,2048]{2,1,0:T(8,128)(2,1)}, u32[]{:S(2)}) copy-start(bf16[8,96,2048]{2,1,0:T(8,128)(2,1)} %all-gather.3.cloned.1.call-done) | copy-start | bytes 9437188
  190.6 5.6 %copy-start.13 = (bf16[128,256]{1,0:T(8,128)(2,1)S(1)}, bf16[128,256]{1,0:T(8,128)(2,1)}, u32[]{:S(2)}) copy-start(bf16[128,256]{1,0:T(8,128)(2,1)} %param.20) | copy-start | bytes 196612
  190.6 6.3 %copy-start.14 = (bf16[128,256]{1,0:T(8,128)(2,1)S(1)}, bf16[128,256]{1,0:T(8,128)(2,1)}, u32[]{:S(2)}) copy-start(bf16[128,256]{1,0:T(8,128)(2,1)} %param.21) | copy-start | bytes 196612
  190.6 5.6 %collective-permute-start.1 = (f32[2,256]{1,0:T(2,128)S(1)}, f32[2,256]{1,0:T(2,128)S(1)}, u32[]{:S(2)}, u32[]{:S(2)}) collective-permute-start(f32[2,256]{1,0:T(2,128)S(1)} %slice.54), channel_id=1, source_target_pairs={{4,0},{8,4},{12,8},{16,12},{20,16},{24,20},{28,24},{5,1},{9,5},{13... | collective-permute-start | bytes 6152 | tf_op jit(solution)/shard_map/ppermute | solution.py:10
Sparse Core Ops, SparseCore 0:
  39.9 27.5 all-gather.2
  69.0 28.4 all-gather.4
  109.1 37.7 reduce-scatter.2
  182.1 62.8 reduce-scatter.4
where the time goes:
time: 254 us; the launch traced here: 253 us
  waiting for transfers between devices  127 us (50%)
  blocking collectives  57.3 us (23%)
  matrix products  34.8 us (14%)
  between operations  14.1 us (6%)
  starting transfers between devices  11 us (4%)
  other arithmetic  6.23 us (2%)
    reduce_scatter x1, waiting for transfers between devices, per_device(): lax.psum_scatter(lax.dot_general(stream_grad, conv_out, contract_first, p...  47.4 us
    reduce_scatter x1, waiting for transfers between devices, per_device(): lax.psum_scatter(row_partial.astype(jnp.bfloat16), 'tp', scatter_dimensio...  37.9 us
    all_to_all x1, blocking collectives, per_device(): lax.all_to_all(sent_rows, 'sp', split_axis=0, concat_axis=0, tiled=True)  27.3 us
    all_to_all x1, blocking collectives, per_device(): lax.all_to_all(sent_cot, 'sp', split_axis=0, concat_axis=0, tiled=True)  23.3 us
    all_gather x1, waiting for transfers between devices, per_device(): lax.all_gather(recv_cot, 'tp', axis=2, tiled=True)  22.2 us
    all_to_all x1, waiting for transfers between devices, per_device(): lax.all_to_all(half_grad, 'sp', split_axis=0, concat_axis=0, tiled=True)  15.2 us
    all_gather x1, blocking collectives, per_device(): moe_grad = lax.all_gather(moe_part, 'tp', axis=1, tiled=True)  6.68 us
    dot_general x1, matrix products, per_device(): lax.dot_general(routed_cot, down_local, contract_last, preferred_element_...  5.69 us
  transfers between devices with their start and end apart: 7, of which 6 were waited for; matrix products, arithmetic and copies ran while one was open for 9% of the time, Pallas kernels for 0%

commit v1 on v0

--- a/solution.py
+++ b/solution.py
@@ -2,6 +2,7 @@
 import jax.numpy as jnp
 from jax import lax
 from jax.sharding import PartitionSpec as P
+from jax.lax import all_gather
 
 
 def from_behind(block, axis, distance):
@@ -60,7 +61,7 @@
     )
     recv_rows, recv_cot = (
         lax.all_gather(recv_rows, "tp", axis=2, tiled=True),
-        lax.all_gather(recv_cot, "tp", axis=2, tiled=True),
+        jnp.concatenate(all_gather(recv_cot, "tp"), axis=2),
     )
     slots = groups * capacity
     routed_rows = recv_rows.reshape(slots, model_width)

time: 254 us -> 258 us (1.016)
  local copies, waits for them, and re-layouts: 2.48 us -> 10.4 us
  matrix products: 34.8 us -> 31.5 us
    reshape x0 -> x1, local copies, waits for them, and re-layouts: none -> 4.32 us  [per_device(): jnp.concatenate(all_gather(recv_cot, 'tp'), axis=2)]
    unnamed x46 -> x55, local copies, waits for them, and re-layouts: 1.45 us -> 5.06 us
    dot_general x1, matrix products: 5.69 us -> 2.31 us  [per_device(): lax.dot_general(routed_cot, down_local, contract_last, preferred_element_...]
where the time goes in v1:
time: 258 us
  waiting for transfers between devices  127 us (49%)
  blocking collectives  57.3 us (22%)
  matrix products  31.5 us (12%)
  between operations  14.1 us (5%)
  starting transfers between devices  11 us (4%)
  local copies, waits for them, and re-layouts  10.4 us (4%)
  other arithmetic  6.23 us (2%)
    reduce_scatter x1, waiting for transfers between devices, per_device(): lax.psum_scatter(lax.dot_general(stream_grad, conv_out, contract_first, p...  47.4 us
    reduce_scatter x1, waiting for transfers between devices, per_device(): lax.psum_scatter(row_partial.astype(jnp.bfloat16), 'tp', scatter_dimensio...  37.9 us
    all_to_all x1, blocking collectives, per_device(): lax.all_to_all(sent_rows, 'sp', split_axis=0, concat_axis=0, tiled=True)  27.3 us
    all_to_all x1, blocking collectives, per_device(): lax.all_to_all(sent_cot, 'sp', split_axis=0, concat_axis=0, tiled=True)  23.3 us
    all_gather x1, waiting for transfers between devices, per_device(): all_gather(recv_cot, 'tp')  22.2 us
    all_to_all x1, waiting for transfers between devices, per_device(): lax.all_to_all(half_grad, 'sp', split_axis=0, concat_axis=0, tiled=True)  15.2 us
    all_gather x1, blocking collectives, per_device(): moe_grad = lax.all_gather(moe_part, 'tp', axis=1, tiled=True)  6.68 us
    all_to_all x1, starting transfers between devices, per_device(): lax.all_to_all(half_grad, 'sp', split_axis=0, concat_axis=0, tiled=True)  5.51 us
  transfers between devices with their start and end apart: 7, of which 6 were waited for; matrix products, arithmetic and copies ran while one was open for 9% of the time, Pallas kernels for 0%

profile of v1, /device:TPU:0, one launch (start us, length us, event | category | flops | bytes accessed | tf_op | source)
XLA Modules:
  0.0 257.8 jit_solution(11165598272904181788)
XLA Ops:
  7.2 0.9 copy.54
  8.5 1.2 reduce-window.6
  10.3 0.7 multiply_add_fusion.1
  11.1 1.2 convolution_convert_fusion.4
  12.4 27.3 %all_to_all.15 = bf16[8,96,512]{2,1,0:T(8,128)(2,1)} all-to-all(bf16[8,96,512]{2,1,0:T(8,128)(2,1)S(1)} %bitcast.82), channel_id=1, replica_groups=mesh['sp'=8,'tp'=4] {'sp'}, dimensions={0} | all-to-all | bytes 1572864 | tf_op jit(solution)/shard_map/all_to_all | solution.py:59
  40.6 23.3 %all_to_all.16 = bf16[8,96,512]{2,1,0:T(8,128)(2,1)} all-to-all(bf16[8,96,512]{2,1,0:T(8,128)(2,1)S(1)} %bitcast.83), channel_id=1, replica_groups=mesh['sp'=8,'tp'=4] {'sp'}, dimensions={0} | all-to-all | bytes 1572864 | tf_op jit(solution)/shard_map/all_to_all | solution.py:60
  63.9 3.5 %all-gather.4.cloned.1.call-done = bf16[8,96,2048]{2,1,0:T(8,128)(2,1)} async-done(((bf16[8,96,512]{2,1,0:T(8,128)(2,1)}), bf16[8,96,2048]{2,1,0:T(8,128)(2,1)}) %all-gather.4.cloned.1.call-update) | async-done | bytes 3145744 | tf_op jit(solution)/shard_map/all_gather | solution.py:63
  67.4 5.0 %fusion.5 = f32[768,512]{1,0:T(8,128)} fusion(bf16[768,2048]{1,0:T(8,128)(2,1)} %bitcast.95, bf16[1,2048,512]{2,1,0:T(8,128)(2,1)S(1)} %copy-done), kind=kOutput, calls=%fused_computation.10 | convolution fusion | flops 1610612736 | bytes 6815744 | tf_op jit(solution)/shard_map/dot_general | solution.py:72
  72.4 2.9 %fusion.8 = f32[768,512]{1,0:T(8,128)} fusion(bf16[768,2048]{1,0:T(8,128)(2,1)S(1)} %bitcast.97, bf16[1,2048,512]{2,1,0:T(8,128)(2,1)S(1)} %copy-done.4), kind=kOutput, calls=%fused_computation.13 | convolution fusion | flops 1610612736 | bytes 6815744 | tf_op jit(solution)/shard_map/dot_general | solution.py:73
  75.3 22.2 %all-gather.6.cloned.1.call-done = bf16[32,96,512]{2,1,0:T(8,128)(2,1)} async-done(((bf16[8,96,512]{2,1,0:T(8,128)(2,1)}), bf16[32,96,512]{2,1,0:T(8,128)(2,1)}) %all-gather.6.cloned.1.call-update) | async-done | bytes 3145744 | tf_op jit(solution)/shard_map/all_gather | solution.py:64
  97.5 4.3 %copy.60 = bf16[8,96,4,512]{3,2,1,0:T(4,128)(2,1)S(1)} copy(bf16[8,96,4,512]{3,1,0,2:T(8,128)(2,1)} %bitcast.81) | data formatting | bytes 6291456 | tf_op jit(solution)/shard_map/reshape | solution.py:64
  101.9 1.0 copy.62
  103.9 1.6 copy-done.24
  105.5 2.3 multiply_convert_fusion.1
  107.9 1.8 fusion.3
  110.0 3.5 %add_convert_fusion = bf16[768,2048]{1,0:T(8,128)(2,1)} fusion(f32[768,2048]{1,0:T(8,128)S(1)} %fusion.3, bf16[768,512]{1,0:T(8,128)(2,1)S(1)} %get-tuple-element.11, bf16[1,2048,512]{2,1,0:T(8,128)(2,1)S(1)} %copy-done.5), kind=kOutput, calls=%fused_computation | convolution fusion | flops 1613758464 | bytes 12320768 | tf_op jit(solution)/shard_map/dot_general | solution.py:96
  113.6 37.9 %reduce-scatter.3.cloned.1.call-done = bf16[768,512]{1,0:T(8,128)(2,1)} async-done(((bf16[768,2048]{1,0:T(8,128)(2,1)}), bf16[768,512]{1,0:T(8,128)(2,1)}) %reduce-scatter.3.cloned.1.call-update) | async-done | bytes 786448 | tf_op jit(solution)/shard_map/reduce_scatter | solution.py:99
  151.5 5.5 %all-to-all-start.2 = ((bf16[8,96,512]{2,1,0:T(8,128)(2,1)}), bf16[8,96,512]{2,1,0:T(8,128)(2,1)S(1)}, u32[]{:S(2)}, u32[]{:S(2)}) async-start(bf16[8,96,512]{2,1,0:T(8,128)(2,1)} %bitcast.87), calls=%async_computation.3 | async-start | bytes 1572864 | tf_op jit(solution)/shard_map/all_to_all | solution.py:104
  157.0 0.9 convert_multiply_fusion.1
  157.9 3.9 %collective-permute-start = (f32[2,256]{1,0:T(2,128)S(1)}, f32[2,256]{1,0:T(2,128)S(1)}, u32[]{:S(2)}, u32[]{:S(2)}) collective-permute-start(f32[2,256]{1,0:T(2,128)S(1)} %slice.49), channel_id=1, source_target_pairs={{0,4},{4,8},{8,12},{12,16},{16,20},{20,24},{24,28},{1,5},{5,9},{9,... | collective-permute-start | bytes 6152 | tf_op jit(solution)/shard_map/ppermute | solution.py:11
  161.9 15.2 %all-to-all-done.2 = bf16[8,96,512]{2,1,0:T(8,128)(2,1)S(1)} async-done(((bf16[8,96,512]{2,1,0:T(8,128)(2,1)}), bf16[8,96,512]{2,1,0:T(8,128)(2,1)S(1)}, u32[]{:S(2)}, u32[]{:S(2)}) %all-to-all-start.2) | async-done | bytes 786464 | tf_op jit(solution)/shard_map/all_to_all | solution.py:104
  177.4 6.7 %all_gather.15 = bf16[128,2048]{1,0:T(8,128)(2,1)S(1)} all-gather(bf16[128,512]{1,0:T(8,128)(2,1)S(1)} %fusion.14), channel_id=1, replica_groups=mesh['sp'=8,'tp'=4] {'tp'}, dimensions={1}, use_global_device_ids=true | all-gather | bytes 655360 | tf_op jit(solution)/shard_map/all_gather | solution.py:110
  184.1 1.0 multiply_convert_fusion.4
  185.1 1.5 convolution_convert_fusion.3
  186.7 5.2 %fusion = bf16[1,2048,512]{2,1,0:T(8,128)(2,1)} fusion(bf16[768,2048]{1,0:T(8,128)(2,1)} %bitcast.96, bf16[768,512]{1,0:T(8,128)(2,1)S(1)} %copy-done.10), kind=kOutput, calls=%fused_computation.4 | convolution fusion | flops 1611661312 | bytes 6029312 | tf_op jit(solution)/shard_map/dot_general | solution.py:84
  191.9 3.3 %fusion.2 = bf16[1,512,2048]{2,1,0:T(8,128)(2,1)} fusion(bf16[768,2048]{1,0:T(8,128)(2,1)S(1)} %bitcast.80, f32[768,512]{1,0:T(8,128)S(1)} %copy-done.25, f32[768,512]{1,0:T(8,128)S(1)} %copy-done.23), kind=kOutput, calls=%fused_computation.6 | convolution fusion | flops 1614020608 | bytes 8388608 | tf_op jit(solution)/shard_map/dot_general | solution.py:90
  195.3 1.4 collective-permute-start.1
  196.7 3.2 %fusion.1 = bf16[1,2048,512]{2,1,0:T(8,128)(2,1)} fusion(bf16[768,2048]{1,0:T(8,128)(2,1)S(1)} %bitcast.98, bf16[768,512]{1,0:T(8,128)(2,1)S(1)} %copy-done.8), kind=kOutput, calls=%fused_computation.5 | convolution fusion | flops 1611661312 | bytes 6029312 | tf_op jit(solution)/shard_map/dot_general | solution.py:87
  199.9 1.0 collective-permute-done.1
  200.9 0.7 fusion.26
  202.2 47.4 %reduce-scatter.5.cloned.1.call-done = bf16[256,256]{1,0:T(8,128)(2,1)} async-done(((bf16[2048,256]{1,0:T(8,128)(2,1)}), bf16[256,256]{1,0:T(8,128)(2,1)}) %reduce-scatter.5.cloned.1.call-update) | async-done | bytes 131088 | tf_op jit(solution)/shard_map/reduce_scatter | solution.py:123
  249.6 1.6 convert_element_type.125
  (86 shorter events, 4.4 us)
Async XLA Ops:
  7.2 60.3 %copy-start = (bf16[1,2048,512]{2,1,0:T(8,128)(2,1)S(1)}, bf16[1,2048,512]{2,1,0:T(8,128)(2,1)}, u32[]{:S(2)}) copy-start(bf16[1,2048,512]{2,1,0:T(8,128)(2,1)} %param.16) | copy-start | bytes 6291460
  7.2 60.3 %all-gather.4.cloned.1.call-start = ((), (), s32[]{:S(2)}) async-start(), calls=%async_computation.5 | async-start | bytes 3932160 | tf_op jit(solution)/shard_map/all_gather | solution.py:63
  11.1 28.7 %copy-start.18 = (f32[128,2]{0,1:T(2,128)S(1)}, f32[128,2]{0,1:T(2,128)}, u32[]{:S(2)}) copy-start(f32[128,2]{0,1:T(2,128)} %param.15) | copy-start | bytes 3076
  11.1 29.1 %copy-start.3 = (bf16[128,2048]{1,0:T(8,128)(2,1)S(1)}, bf16[128,2048]{1,0:T(8,128)(2,1)}, u32[]{:S(2)}) copy-start(bf16[128,2048]{1,0:T(8,128)(2,1)} %param.12) | copy-start | bytes 1572868
  39.7 57.8 %all-gather.6.cloned.1.call-start = ((), (), s32[]{:S(2)}) async-start(), calls=%async_computation.8 | async-start | bytes 3932160 | tf_op jit(solution)/shard_map/all_gather | solution.py:64
  63.9 87.6 %reduce-scatter.3.cloned.1.call-start = ((), (), s32[]{:S(2)}) async-start(), calls=%async_computation.6 | async-start | bytes 3932160 | tf_op jit(solution)/shard_map/reduce_scatter | solution.py:99
  67.4 5.0 %copy-start.4 = (bf16[1,2048,512]{2,1,0:T(8,128)(2,1)S(1)}, bf16[1,2048,512]{2,1,0:T(8,128)(2,1)}, u32[]{:S(2)}) copy-start(bf16[1,2048,512]{2,1,0:T(8,128)(2,1)} %param.17) | copy-start | bytes 6291460
  67.4 5.0 %copy-start.19 = (bf16[8,96,2048]{2,1,0:T(8,128)(2,1)S(1)}, bf16[8,96,2048]{2,1,0:T(8,128)(2,1)}, u32[]{:S(2)}) copy-start(bf16[8,96,2048]{2,1,0:T(8,128)(2,1)} %all-gather.4.cloned.1.call-done) | copy-start | bytes 9437188
  101.9 1.6 copy-start.21
  101.9 2.1 copy-start.22
  101.9 3.6 %copy-start.24 = (f32[768,512]{1,0:T(8,128)S(1)}, f32[768,512]{1,0:T(8,128)}, u32[]{:S(2)}) copy-start(f32[768,512]{1,0:T(8,128)} %fusion.8) | copy-start | bytes 4718596
  102.9 4.9 %copy-start.1 = (bf16[96,8,4,512]{3,1,2,0:T(8,128)(2,1)}, bf16[96,8,4,512]{3,1,2,0:T(8,128)(2,1)S(1)}, u32[]{:S(2)}) copy-start(bf16[96,8,4,512]{3,1,2,0:T(8,128)(2,1)S(1)} %copy.62) | copy-start | bytes 9437188
  107.8 1.9 copy-start.9
  107.9 1.9 copy-start.7
  107.9 2.2 copy-start.5
  113.6 48.3 %copy-start.17 = (bf16[3,256]{1,0:T(4,128)(2,1)S(1)}, bf16[3,256]{1,0:T(4,128)(2,1)}, u32[]{:S(2)}) copy-start(bf16[3,256]{1,0:T(4,128)(2,1)} %param.22) | copy-start | bytes 4612
  151.5 25.6 %all-to-all-start.2 = ((bf16[8,96,512]{2,1,0:T(8,128)(2,1)}), bf16[8,96,512]{2,1,0:T(8,128)(2,1)S(1)}, u32[]{:S(2)}, u32[]{:S(2)}) async-start(bf16[8,96,512]{2,1,0:T(8,128)(2,1)} %bitcast.87), calls=%async_computation.3 | async-start | bytes 1572864 | tf_op jit(solution)/shard_map/all_to_all | solution.py:104
  157.0 92.7 %reduce-scatter.5.cloned.1.call-start = ((), (), s32[]{:S(2)}) async-start(), calls=%async_computation.7 | async-start | bytes 1179648 | tf_op jit(solution)/shard_map/reduce_scatter | solution.py:123
  157.9 3.9 %copy-start.12 = (f32[128,256]{1,0:T(8,128)}, f32[128,256]{1,0:T(8,128)S(1)}, u32[]{:S(2)}) copy-start(f32[128,256]{1,0:T(8,128)S(1)} %convert_multiply_fusion.1) | copy-start | bytes 393220
  157.9 26.2 %collective-permute-start = (f32[2,256]{1,0:T(2,128)S(1)}, f32[2,256]{1,0:T(2,128)S(1)}, u32[]{:S(2)}, u32[]{:S(2)}) collective-permute-start(f32[2,256]{1,0:T(2,128)S(1)} %slice.49), channel_id=1, source_target_pairs={{0,4},{4,8},{8,12},{12,16},{16,20},{20,24},{24,28},{1,5},{5,9},{9,... | collective-permute-start | bytes 6152 | tf_op jit(solution)/shard_map/ppermute | solution.py:11
  177.1 7.1 %copy-start.6 = (bf16[2048,256]{1,0:T(8,128)(2,1)S(1)}, bf16[2048,256]{1,0:T(8,128)(2,1)}, u32[]{:S(2)}) copy-start(bf16[2048,256]{1,0:T(8,128)(2,1)} %param.23) | copy-start | bytes 3145732
  177.1 7.1 %copy-start.13 = (f32[128,256]{1,0:T(8,128)S(1)}, f32[128,256]{1,0:T(8,128)}, u32[]{:S(2)}) copy-start(f32[128,256]{1,0:T(8,128)} %copy-done.12) | copy-start | bytes 393220
  177.1 7.1 %copy-start.14 = (bf16[128,256]{1,0:T(8,128)(2,1)S(1)}, bf16[128,256]{1,0:T(8,128)(2,1)}, u32[]{:S(2)}) copy-start(bf16[128,256]{1,0:T(8,128)(2,1)} %param.19) | copy-start | bytes 196612
  186.7 5.2 %copy-start.2 = (bf16[96,8,4,512]{3,1,2,0:T(8,128)(2,1)S(1)}, bf16[96,8,4,512]{3,1,2,0:T(8,128)(2,1)}, u32[]{:S(2)}) copy-start(bf16[96,8,4,512]{3,1,2,0:T(8,128)(2,1)} %copy-done.1) | copy-start | bytes 9437188
  186.7 5.2 %copy-start.23 = (f32[768,512]{1,0:T(8,128)S(1)}, f32[768,512]{1,0:T(8,128)}, u32[]{:S(2)}) copy-start(f32[768,512]{1,0:T(8,128)} %fusion.5) | copy-start | bytes 4718596
  186.7 5.2 %copy-start.25 = (f32[768,512]{1,0:T(8,128)S(1)}, f32[768,512]{1,0:T(8,128)}, u32[]{:S(2)}) copy-start(f32[768,512]{1,0:T(8,128)} %fusion.8) | copy-start | bytes 4718596
  191.9 3.3 %copy-start.11 = (f32[128,256]{1,0:T(8,128)S(1)}, f32[128,256]{1,0:T(8,128)}, u32[]{:S(2)}) copy-start(f32[128,256]{1,0:T(8,128)} %get-tuple-element.13) | copy-start | bytes 393220
  191.9 4.8 %copy-start.8 = (bf16[768,512]{1,0:T(8,128)(2,1)S(1)}, bf16[768,512]{1,0:T(8,128)(2,1)}, u32[]{:S(2)}) copy-start(bf16[768,512]{1,0:T(8,128)(2,1)} %copy-done.7) | copy-start | bytes 2359300
  191.9 4.8 %copy-start.20 = (bf16[8,96,2048]{2,1,0:T(8,128)(2,1)S(1)}, bf16[8,96,2048]{2,1,0:T(8,128)(2,1)}, u32[]{:S(2)}) copy-start(bf16[8,96,2048]{2,1,0:T(8,128)(2,1)} %all-gather.4.cloned.1.call-done) | copy-start | bytes 9437188
  195.3 5.6 %copy-start.15 = (bf16[128,256]{1,0:T(8,128)(2,1)S(1)}, bf16[128,256]{1,0:T(8,128)(2,1)}, u32[]{:S(2)}) copy-start(bf16[128,256]{1,0:T(8,128)(2,1)} %param.20) | copy-start | bytes 196612
  195.3 6.3 %copy-start.16 = (bf16[128,256]{1,0:T(8,128)(2,1)S(1)}, bf16[128,256]{1,0:T(8,128)(2,1)}, u32[]{:S(2)}) copy-start(bf16[128,256]{1,0:T(8,128)(2,1)} %param.21) | copy-start | bytes 196612
  195.3 5.6 %collective-permute-start.1 = (f32[2,256]{1,0:T(2,128)S(1)}, f32[2,256]{1,0:T(2,128)S(1)}, u32[]{:S(2)}, u32[]{:S(2)}) collective-permute-start(f32[2,256]{1,0:T(2,128)S(1)} %slice.54), channel_id=1, source_target_pairs={{4,0},{8,4},{12,8},{16,12},{20,16},{24,20},{28,24},{5,1},{9,5},{13... | collective-permute-start | bytes 6152 | tf_op jit(solution)/shard_map/ppermute | solution.py:11
  (1 other events, 1.5 us)
Sparse Core Ops, SparseCore 0:
  39.9 27.5 all-gather.3
  69.0 28.4 all-gather.5
  113.7 37.7 reduce-scatter.2
  186.8 62.8 reduce-scatter.4
